TPU v7x, 32 devices: a whole 2x2x4 slice. The times are simulated.
32 devices in a mesh: grp: 2 (over y), sp: 8 (over z, core), tp: 2 (over x).
Axes of the slice: x: 2, y: 2, z: 4, core: 2. Of those that a mesh axis runs over, the one named last changes fastest.
Arguments:
- queries: bfloat16 [12288, 1024], P(('grp', 'sp'), 'tp'), parts along dimension 0, may hold values from -200 to 200
- key_rows: bfloat16 [12288, 512], P(('grp', 'sp'), 'tp'), parts along dimension 0, may hold values from -6 to 6
- value_rows: bfloat16 [12288, 512], P(('grp', 'sp'), 'tp'), parts along dimension 0, may hold values from -6 to 6
- doc_ids: int32 [12288], P(('grp', 'sp')), parts along dimension 0, may hold values from 0 to 3, never falling along the last dimension, each value on 1 to 3072 neighbouring positions
- sink_logits: float32 [16], P('tp'), may hold values from 2 to 7
- out_weight: bfloat16 [1024, 2048], P('tp', 'sp'), may hold values from -0.1875 to 0.1875
- residual: bfloat16 [12288, 2048], P(('grp', 'sp', 'tp')), parts along dimension 0, may hold values from -6 to 6
- gain_mixed: float32 [2048], replicated, may hold values from 0.1 to 1.9
- gain_before: float32 [2048], replicated, may hold values from 0.1 to 1.9
- gain_after: float32 [2048], replicated, may hold values from 0.1 to 1.9
- gate_weight: bfloat16 [2048, 6144], P('sp', 'tp'), may hold values from -0.125 to 0.125
- up_weight: bfloat16 [2048, 6144], P('sp', 'tp'), may hold values from -0.125 to 0.125
- down_weight: bfloat16 [6144, 2048], P('tp', 'sp'), may hold values from -0.078125 to 0.078125
Outputs:
- layer_out: bfloat16 [12288, 2048], P(('grp', 'sp', 'tp')), parts along dimension 0
There are 2 independent parts, one for each index of `grp`. A program takes and returns all parts, laid end to end along the dimension named above; an argument that names none is the same for every part. Nothing has to cross between parts.
All inputs are finite; a program needn't handle non-finite values.
Results may differ from a plain program's by a relative error of at most 0.015.
Values may be sent and summed in bfloat16 or wider, within the bound.
A program may use at most 128 MiB of HBM per device.

v0:
```python
import jax
import jax.numpy as jnp
from jax import lax
from jax.sharding import PartitionSpec as P

HEAD_DIM = 64
WINDOW = 128


epsilon = 1e-06
masked_value = -1e30


def passed_along(value, axis, steps):
    count = lax.axis_size(axis)
    first, last = (max(0, -steps), min(count, count - steps))
    return lax.ppermute(value, axis, [(source, source + steps) for source in range(first, last)])


def stored(value):
    return lax.optimization_barrier(value.astype(jnp.bfloat16)).astype(jnp.float32)


def rms_scaled(value, gain):
    return value * lax.rsqrt(jnp.mean(value * value, axis=-1, keepdims=True) + epsilon) * gain


def windows(array, blocks):
    first = array[:-WINDOW].reshape((blocks, WINDOW) + array.shape[1:])
    second = array[WINDOW:].reshape((blocks, WINDOW) + array.shape[1:])
    return jnp.concatenate([first, second], axis=1)


def attend(queries, key_rows, value_rows, doc_ids, sink_logits):
    length = queries.shape[0]
    blocks = length // WINDOW
    local_kv = key_rows.shape[1] // HEAD_DIM
    group_size = queries.shape[1] // HEAD_DIM // local_kv
    offset = lax.axis_index("sp") * length
    tail_keys, tail_values, tail_docs = passed_along(
        (key_rows[length - WINDOW :], value_rows[length - WINDOW :], doc_ids[length - WINDOW :]),
        "sp",
        1,
    )
    key_blocks = windows(jnp.concatenate([tail_keys, key_rows], axis=0), blocks).reshape(
        blocks, 2 * WINDOW, local_kv, HEAD_DIM
    )
    value_blocks = windows(jnp.concatenate([tail_values, value_rows], axis=0), blocks).reshape(
        blocks, 2 * WINDOW, local_kv, HEAD_DIM
    )
    key_docs = windows(jnp.concatenate([tail_docs, doc_ids], axis=0), blocks)
    key_places = windows(offset - WINDOW + jnp.arange(length + WINDOW, dtype=jnp.int32), blocks)
    query_places = (offset + jnp.arange(length, dtype=jnp.int32)).reshape(blocks, WINDOW)
    query_docs = doc_ids.reshape(blocks, WINDOW)
    query_blocks = queries.reshape(blocks, WINDOW, local_kv, group_size, HEAD_DIM)
    scores = jnp.einsum(
        "bqhgd,bkhd->bhgqk", query_blocks, key_blocks, preferred_element_type=jnp.float32
    ) * HEAD_DIM ** (-0.5)
    distance = query_places[:, :, None] - key_places[:, None, :]
    valid = (distance >= 0) & (distance < WINDOW) & (key_places[:, None, :] >= 0)
    valid = valid & (query_docs[:, :, None] == key_docs[:, None, :])
    scores = jnp.where(valid[:, None, None], scores, masked_value)
    sinks = sink_logits.reshape(local_kv, group_size)[None, :, :, None]
    top = jnp.maximum(jnp.max(scores, axis=-1), sinks)
    weight = jnp.exp(scores - top[..., None])
    denom = jnp.sum(weight, axis=-1) + jnp.exp(sinks - top)
    summed = jnp.einsum(
        "bhgqk,bkhd->bqhgd",
        weight.astype(jnp.bfloat16),
        value_blocks,
        preferred_element_type=jnp.float32,
    )
    scale = jnp.transpose(denom, (0, 3, 1, 2))[..., None]
    return (summed / scale).reshape(length, queries.shape[1]).astype(jnp.bfloat16)


def per_device(
    queries,
    key_rows,
    value_rows,
    doc_ids,
    sink_logits,
    out_weight,
    residual,
    gain_mixed,
    gain_before,
    gain_after,
    gate_weight,
    up_weight,
    down_weight,
):
    mixed = attend(queries, key_rows, value_rows, doc_ids, sink_logits)
    head_columns = lax.all_gather(out_weight, "sp", axis=1, tiled=True)
    projected = lax.psum_scatter(
        jnp.dot(mixed, head_columns, preferred_element_type=jnp.float32).astype(jnp.bfloat16),
        "tp",
        scatter_dimension=0,
        tiled=True,
    ).astype(jnp.float32)
    projected = stored(projected)
    after = stored(residual.astype(jnp.float32) + rms_scaled(projected, gain_mixed))
    normed = rms_scaled(after, gain_before).astype(jnp.bfloat16)
    full_gate, full_up, full_down = (
        lax.all_gather(gate_weight, "sp", axis=0, tiled=True),
        lax.all_gather(up_weight, "sp", axis=0, tiled=True),
        lax.all_gather(down_weight, "sp", axis=1, tiled=True),
    )
    piece = lax.all_gather(normed, "tp", axis=0, tiled=True)
    gate = jnp.dot(piece, full_gate, preferred_element_type=jnp.float32)
    upward = jnp.dot(piece, full_up, preferred_element_type=jnp.float32)
    hidden = (jax.nn.silu(gate) * upward).astype(jnp.bfloat16)
    ffn_out = stored(
        lax.psum_scatter(
            jnp.dot(hidden, full_down, preferred_element_type=jnp.float32).astype(jnp.bfloat16),
            "tp",
            scatter_dimension=0,
            tiled=True,
        ).astype(jnp.float32)
    )
    return (after + 0.5 * rms_scaled(ffn_out, gain_after)).astype(jnp.bfloat16)


def solution(mesh):
    return jax.shard_map(
        per_device,
        mesh=mesh,
        in_specs=(
            P(("grp", "sp"), "tp"),
            P(("grp", "sp"), "tp"),
            P(("grp", "sp"), "tp"),
            P(("grp", "sp")),
            P("tp"),
            P("tp", "sp"),
            P(("grp", "sp", "tp"), None),
            P(),
            P(),
            P(),
            P("sp", "tp"),
            P("sp", "tp"),
            P("tp", "sp"),
        ),
        out_specs=P(("grp", "sp", "tp"), None),
        check_vma=False,
    )
```

profile of v0, /device:TPU:0, one launch (start us, length us, event | category | flops | bytes accessed | tf_op | source)
XLA Modules:
  0.0 577.6 jit_solution(4253527668909372230)
XLA Ops:
  6.5 0.7 all-gather.6.cloned.1.call-update
  7.3 0.0 reduce-scatter.3.cloned.1.call-start
  7.3 0.7 slice.40
  8.0 2.4 collective-permute-start.1
  10.4 0.8 slice.43
  11.2 5.2 collective-permute-start.2
  16.4 0.8 slice.36
  17.3 1.3 collective-permute-start
  18.7 1.8 reshape.107
  20.5 0.0 copy-start.8
  20.5 0.0 copy-start
  20.5 1.9 reshape.105
  22.4 1.7 reshape.108
  24.1 1.1 copy.23
  25.2 0.1 max.16
  25.3 1.1 copy.19
  26.4 0.0 collective-permute-done.1
  26.4 1.0 fusion.33
  27.4 0.0 copy-start.2
  27.4 0.0 collective-permute-done.2
  27.4 1.0 pad_maximum_fusion
  28.4 0.3 reshape.106
  28.7 0.0 copy-start.6
  28.7 1.1 copy.22
  29.8 0.0 collective-permute-done
  29.9 0.3 reshape.104
  30.2 1.1 copy.18
  31.3 0.0 copy-done.2
  31.3 2.3 fusion.2
  33.6 0.1 broadcast_maximum_fusion
  33.7 0.0 copy-start.7
  33.7 1.7 fusion
  35.4 0.1 add_bitcast_fusion
  35.5 1.6 fusion.20
  37.1 0.6 copy.27
  37.7 4.6 all-gather.6.cloned.1.call-done
  42.2 5.1 convolution_convert_fusion
  47.3 0.0 reduce-scatter.3.cloned.1.call-update
  47.3 0.0 all-gather.8.cloned.1.call-start
  47.4 42.3 %reduce-scatter.3.cloned.1.call-done = bf16[384,2048]{1,0:T(8,128)(2,1)} async-done(((bf16[768,2048]{1,0:T(8,128)(2,1)}), bf16[384,2048]{1,0:T(8,128)(2,1)}) %reduce-scatter.3.cloned.1.call-update) | async-done | bytes 1572880 | tf_op jit(solution)/shard_map/reduce_scatter | solution.py:94
  89.6 1.8 fusion.3
  91.5 0.0 copy-start.10
  91.5 2.2 fusion.6
  93.7 0.4 fusion.10
  94.1 1.6 fusion.12
  95.7 0.0 all-gather.8.cloned.1.call-update
  95.7 0.0 all-gather.10.cloned.1.call-start
  95.8 0.5 all-gather.10.cloned.1.call-update
  96.3 0.0 all-gather.12.cloned.1.call-start
  96.3 0.5 all-gather.12.cloned.1.call-update
  96.9 0.0 all-gather.14.cloned.1.call-start
  96.9 0.5 all-gather.14.cloned.1.call-update
  97.4 0.2 reduce-scatter.5.cloned.1.call-start
  97.7 43.1 %all-gather.8.cloned.1.call-done = bf16[768,2048]{1,0:T(8,128)(2,1)} async-done(((bf16[384,2048]{1,0:T(8,128)(2,1)}), bf16[768,2048]{1,0:T(8,128)(2,1)}) %all-gather.8.cloned.1.call-update) | async-done | bytes 3145744 | tf_op jit(solution)/shard_map/all_gather | solution.py:108
  140.8 118.2 %all-gather.10.cloned.1.call-done = bf16[2048,3072]{1,0:T(8,128)(2,1)} async-done(((bf16[256,3072]{1,0:T(8,128)(2,1)}), bf16[2048,3072]{1,0:T(8,128)(2,1)}) %all-gather.10.cloned.1.call-update) | async-done | bytes 12582928 | tf_op jit(solution)/shard_map/all_gather | solution.py:104
  259.0 16.0 %fusion.39 = f32[768,3072]{1,0:T(8,128)} fusion(bf16[768,2048]{1,0:T(8,128)(2,1)} %all-gather.8.cloned.1.call-done, bf16[2048,3072]{1,0:T(8,128)(2,1)} %all-gather.10.cloned.1.call-done), kind=kOutput, calls=%fused_computation.67 | convolution fusion | flops 9663676416 | bytes 25165824 | tf_op jit(solution)/shard_map/dot_general | solution.py:109
  275.0 100.4 %all-gather.12.cloned.1.call-done = bf16[2048,3072]{1,0:T(8,128)(2,1)} async-done(((bf16[256,3072]{1,0:T(8,128)(2,1)}), bf16[2048,3072]{1,0:T(8,128)(2,1)}) %all-gather.12.cloned.1.call-update) | async-done | bytes 12582928 | tf_op jit(solution)/shard_map/all_gather | solution.py:105
  375.4 116.8 %all-gather.14.cloned.1.call-done = bf16[3072,2048]{1,0:T(8,128)(2,1)} async-done(((bf16[3072,256]{1,0:T(8,128)(2,1)}), bf16[3072,2048]{1,0:T(8,128)(2,1)}) %all-gather.14.cloned.1.call-update) | async-done | bytes 12582928 | tf_op jit(solution)/shard_map/all_gather | solution.py:106
  492.2 31.5 %convolution_convert_fusion.1 = bf16[768,2048]{1,0:T(8,128)(2,1)} fusion(bf16[3072,2048]{1,0:T(8,128)(2,1)} %all-gather.14.cloned.1.call-done, f32[768,3072]{1,0:T(8,128)} %fusion.39, bf16[768,2048]{1,0:T(8,128)(2,1)} %all-gather.8.cloned.1.call-done, bf16[2048,3072]{1,0:T(8,128)(2,1)} %all-gather.12.cloned.1.call-done), kind=kOutput, calls=%fused_computation.14 | convolution fusion | flops 19343081472 | bytes 40894464 | tf_op jit(solution)/shard_map/dot_general | solution.py:114
  523.8 0.0 reduce-scatter.5.cloned.1.call-update
  523.8 41.8 %reduce-scatter.5.cloned.1.call-done = bf16[384,2048]{1,0:T(8,128)(2,1)} async-done(((bf16[768,2048]{1,0:T(8,128)(2,1)}), bf16[384,2048]{1,0:T(8,128)(2,1)}) %reduce-scatter.5.cloned.1.call-update) | async-done | bytes 1572880 | tf_op jit(solution)/shard_map/reduce_scatter | solution.py:113
  565.6 1.8 fusion.7
  567.4 0.0 copy-done.11
  567.4 3.4 fusion.13
  (30 shorter events, 0.1 us)
Async XLA Ops:
  6.5 15.9 %copy-start.4 = (bf16[768,512]{1,0:T(8,128)(2,1)S(1)}, bf16[768,512]{1,0:T(8,128)(2,1)}, u32[]{:S(2)}) copy-start(bf16[768,512]{1,0:T(8,128)(2,1)} %param.13) | copy-start | bytes 2359300
  6.5 35.7 %all-gather.6.cloned.1.call-start = ((), (), s32[]{:S(2)}) async-start(), calls=%async_computation.2 | async-start | bytes 2359296 | tf_op jit(solution)/shard_map/all_gather | solution.py:93
  7.3 18.0 %copy-start.12 = (f32[8]{0:T(128)S(1)}, f32[8]{0:T(128)}, u32[]{:S(2)}) copy-start(f32[8]{0:T(128)} %param.17) | copy-start | bytes 100
  7.3 82.4 %reduce-scatter.3.cloned.1.call-start = ((), (), s32[]{:S(2)}) async-start(), calls=%async_computation.3 | async-start | bytes 4718592 | tf_op jit(solution)/shard_map/reduce_scatter | solution.py:94
  8.0 18.4 %collective-permute-start.1 = (s32[128]{0:T(128)S(1)}, s32[128]{0:T(128)S(1)}, u32[]{:S(2)}, u32[]{:S(2)}) collective-permute-start(s32[128]{0:T(128)S(1)} %slice.40), channel_id=1, source_target_pairs={{0,2},{2,4},{4,6},{6,8},{8,10},{10,12},{12,14},{1,3},{3,5},{5,7},{... | collective-permute-start | bytes 1544 | tf_op jit(solution)/shard_map/ppermute | solution.py:17
  11.2 16.2 %collective-permute-start.2 = (bf16[128,256]{1,0:T(8,128)(2,1)S(1)}, bf16[128,256]{1,0:T(8,128)(2,1)}, u32[]{:S(2)}, u32[]{:S(2)}) collective-permute-start(bf16[128,256]{1,0:T(8,128)(2,1)S(1)} %slice.43), channel_id=1, source_target_pairs={{0,2},{2,4},{4,6},{6,8},{8,10},{10,12},{12,14},{1,3},{3,5},{5,7},{... | collective-permute-start | bytes 196616 | tf_op jit(solution)/shard_map/ppermute | solution.py:17
  17.3 12.6 %collective-permute-start = (bf16[128,256]{1,0:T(8,128)(2,1)S(1)}, bf16[128,256]{1,0:T(8,128)(2,1)S(1)}, u32[]{:S(2)}, u32[]{:S(2)}) collective-permute-start(bf16[128,256]{1,0:T(8,128)(2,1)S(1)} %slice.36), channel_id=1, source_target_pairs={{0,2},{2,4},{4,6},{6,8},{8,10},{10,12},{12,14},{1,3},{3,5},{5,7},{... | collective-permute-start | bytes 196616 | tf_op jit(solution)/shard_map/ppermute | solution.py:17
  20.5 5.9 %copy-start.8 = (s32[768]{0:T(1024)S(1)}, s32[768]{0:T(1024)}, u32[]{:S(2)}) copy-start(s32[768]{0:T(1024)} %param.16) | copy-start | bytes 9220
  20.5 6.9 %copy-start = (bf16[768,256]{1,0:T(8,128)(2,1)S(1)}, bf16[768,256]{1,0:T(8,128)(2,1)}, u32[]{:S(2)}) copy-start(bf16[768,256]{1,0:T(8,128)(2,1)} %param.14) | copy-start | bytes 1179652
  24.1 5.7 copy-start.1
  27.4 3.9 copy-start.2
  28.7 2.6 copy-start.6
  33.7 1.8 copy-start.5
  33.7 1.8 copy-start.7
  47.3 44.1 %copy-start.3 = (bf16[384,2048]{1,0:T(8,128)(2,1)S(1)}, bf16[384,2048]{1,0:T(8,128)(2,1)}, u32[]{:S(2)}) copy-start(bf16[384,2048]{1,0:T(8,128)(2,1)} %param.19) | copy-start | bytes 4718596
  47.3 44.1 %copy-start.9 = (f32[2048]{0:T(1024)S(1)}, f32[2048]{0:T(1024)}, u32[]{:S(2)}) copy-start(f32[2048]{0:T(1024)} %param.20) | copy-start | bytes 24580
  47.3 93.4 %all-gather.8.cloned.1.call-start = ((), (), s32[]{:S(2)}) async-start(), calls=%async_computation.4 | async-start | bytes 4718592 | tf_op jit(solution)/shard_map/all_gather | solution.py:108
  91.5 2.7 copy-start.10
  95.7 163.3 %all-gather.10.cloned.1.call-start = ((), (), s32[]{:S(2)}) async-start(), calls=%async_computation.5 | async-start | bytes 14155776 | tf_op jit(solution)/shard_map/all_gather | solution.py:104
  96.3 279.2 %all-gather.12.cloned.1.call-start = ((), (), s32[]{:S(2)}) async-start(), calls=%async_computation.6 | async-start | bytes 14155776 | tf_op jit(solution)/shard_map/all_gather | solution.py:105
  96.9 395.4 %all-gather.14.cloned.1.call-start = ((), (), s32[]{:S(2)}) async-start(), calls=%async_computation.7 | async-start | bytes 14155776 | tf_op jit(solution)/shard_map/all_gather | solution.py:106
  97.4 468.1 %reduce-scatter.5.cloned.1.call-start = ((), (), s32[]{:S(2)}) async-start(), calls=%async_computation.8 | async-start | bytes 4718592 | tf_op jit(solution)/shard_map/reduce_scatter | solution.py:113
  523.8 43.6 %copy-start.11 = (f32[2048]{0:T(1024)S(1)}, f32[2048]{0:T(1024)}, u32[]{:S(2)}) copy-start(f32[2048]{0:T(1024)} %param.22) | copy-start | bytes 24580
Sparse Core Ops, SparseCore 0:
  8.9 33.2 all-gather.5
  47.5 42.1 reduce-scatter.2
  95.8 44.9 all-gather.7
  142.3 116.6 all-gather.9
  260.5 114.8 all-gather.11
  376.9 115.3 all-gather.13
  523.9 41.6 reduce-scatter.4
where the time goes:
time: 578 us
  waiting for transfers between devices  469 us (81%)
  matrix products  56.5 us (10%)
  other arithmetic  15.1 us (3%)
  between operations  13.8 us (2%)
  local copies, waits for them, and re-layouts  13.5 us (2%)
  starting transfers between devices  9.3 us (2%)
    all_gather x1, waiting for transfers between devices, per_device(): lax.all_gather(gate_weight, 'sp', axis=0, tiled=True)  118 us
    all_gather x1, waiting for transfers between devices, per_device(): lax.all_gather(down_weight, 'sp', axis=1, tiled=True)  117 us
    all_gather x1, waiting for transfers between devices, per_device(): lax.all_gather(up_weight, 'sp', axis=0, tiled=True)  100 us
    all_gather x1, waiting for transfers between devices, per_device(): piece = lax.all_gather(normed, 'tp', axis=0, tiled=True)  43.1 us
    reduce_scatter x1, waiting for transfers between devices, per_device(): lax.psum_scatter(jnp.dot(mixed, head_columns, preferred_element_type=jnp....  42.3 us
    reduce_scatter x1, waiting for transfers between devices, per_device(): lax.psum_scatter(jnp.dot(hidden, full_down, preferred_element_type=jnp.fl...  41.8 us
    dot_general x1, matrix products, per_device(): jnp.dot(hidden, full_down, preferred_element_type=jnp.float32)  31.5 us
    dot_general x1, matrix products, per_device(): gate = jnp.dot(piece, full_gate, preferred_element_type=jnp.float32)  16 us
  transfers between devices with their start and end apart: 10, of which 7 were waited for; matrix products, arithmetic and copies ran while one was open for 6% of the time, Pallas kernels for 0%

commit v1 on v0

--- a/solution.py
+++ b/solution.py
@@ -1,6 +1,10 @@
+import functools
+
 import jax
 import jax.numpy as jnp
 from jax import lax
+from jax.experimental import pallas as pl
+from jax.experimental.pallas import tpu as pltpu
 from jax.sharding import PartitionSpec as P
 
 HEAD_DIM = 64
@@ -73,6 +77,346 @@
     scale = jnp.transpose(denom, (0, 3, 1, 2))[..., None]
     return (summed / scale).reshape(length, queries.shape[1]).astype(jnp.bfloat16)
 
+MESH = pl.DeviceIdType.MESH
+PHASES = 4
+
+
+def block_kernel(
+    levels, mixed, wout, resid, gain_m, gain_b, gain_a, gate, up, down, out,
+    full_gate, full_up, full_down, psend, precv, after, normed, hidden, fsend, frecv, fown,
+    z_recv, z_up, z_dn, y_send, y_recv, c_send, c_recv, own_sem, x_send, x_recv, f_send, f_recv,
+):
+    y, s, x = lax.axis_index("grp"), lax.axis_index("sp"), lax.axis_index("tp")
+    z, c = s // 2, s % 2
+    y_peer, x_peer, c_peer = {"grp": 1 - y}, {"tp": 1 - x}, {"sp": z * 2 + 1 - c}
+    above, below = {"sp": jnp.minimum(s + 2, 2 * levels - 1)}, {"sp": jnp.maximum(s - 2, 0)}
+    half_rows = gate.shape[0] // 2
+    down_rows = down.shape[0] // 2
+    width = down.shape[1] // 2
+    mine = resid.shape[0]
+    dim = resid.shape[1]
+    own_rows, peer_rows = pl.ds(pl.multiple_of(x * mine, mine), mine), pl.ds(pl.multiple_of((1 - x) * mine, mine), mine)
+
+    barrier = pltpu.get_barrier_semaphore()
+
+    def greet(device):
+        pl.semaphore_signal(barrier, inc=1, device_id=device, device_id_type=MESH)
+
+    greet(y_peer)
+    greet(x_peer)
+    greet(c_peer)
+
+    @pl.when(z < levels - 1)
+    def _():
+        greet(above)
+
+    @pl.when(z > 0)
+    def _():
+        greet(below)
+
+    neighbours = jnp.where(z > 0, 1, 0) + jnp.where(z < levels - 1, 1, 0)
+    pl.semaphore_wait(barrier, 3 + neighbours)
+
+    def place(q, zz, cc, hh):
+        if q < 2:
+            row = pl.multiple_of(((zz * 2 + cc) * 2 + hh) * half_rows, half_rows)
+            return (full_gate, full_up)[q].at[pl.ds(row, half_rows), :]
+        return full_down.at[
+            q - 2, zz, pl.ds(pl.multiple_of(hh * down_rows, down_rows), down_rows), pl.ds(pl.multiple_of(cc * width, width), width)
+        ]
+
+    def piece(q, hh):
+        if q < 2:
+            return (gate, up)[q].at[pl.ds(pl.multiple_of(hh * half_rows, half_rows), half_rows), :]
+        return down.at[pl.ds(pl.multiple_of(hh * down_rows, down_rows), down_rows), pl.ds((q - 2) * width, width)]
+
+    def remote(source, target, send, recv, device):
+        return pltpu.make_async_remote_copy(
+            src_ref=source, dst_ref=target, send_sem=send, recv_sem=recv, device_id=device, device_id_type=MESH
+        )
+
+    def upward(q, zz, source):
+        return remote(source, place(q, zz, c, y), z_up.at[q, zz], z_recv.at[q, zz], above)
+
+    def downward(q, zz, source):
+        return remote(source, place(q, zz, c, y), z_dn.at[q, zz], z_recv.at[q, zz], below)
+
+    def across(q, zz):
+        block = place(q, zz, c, y)
+        return remote(block, block, y_send.at[q, zz], y_recv.at[q, zz], y_peer)
+
+    def arrived_across(q, zz):
+        block = place(q, zz, c, 1 - y)
+        return remote(block, block, y_send.at[q, zz], y_recv.at[q, zz], y_peer)
+
+    def beside(q, zz, hh, cc, source=None):
+        block = place(q, zz, cc, hh)
+        return remote(block if source is None else source, block, c_send.at[q, zz, hh], c_recv.at[q, zz, hh], c_peer)
+
+    def keep(q, hh):
+        return pltpu.make_async_copy(piece(q, hh), place(q, z, c, hh), own_sem.at[q, hh])
+
+    def own(q):
+        @pl.when(z < levels - 1)
+        def _():
+            upward(q, z, piece(q, y)).start()
+
+        @pl.when(z > 0)
+        def _():
+            downward(q, z, piece(q, y)).start()
+
+        for hh in range(2):
+            beside(q, z, hh, c, piece(q, hh)).start()
+            keep(q, hh).start()
+
+    def from_line(q, t):
+        low, high = z - t, z + t
+
+        @pl.when(low >= 0)
+        def _():
+            upward(q, low, place(q, low, c, y)).wait_recv()
+
+            @pl.when(z < levels - 1)
+            def _():
+                upward(q, low, place(q, low, c, y)).start()
+
+            across(q, low).start()
+            beside(q, low, y, c).start()
+
+        @pl.when(high < levels)
+        def _():
+            downward(q, high, place(q, high, c, y)).wait_recv()
+
+            @pl.when(z > 0)
+            def _():
+                downward(q, high, place(q, high, c, y)).start()
+
+            across(q, high).start()
+            beside(q, high, y, c).start()
+
+    def from_side(q, t):
+        for zz, there in ((z - t, z - t >= 0), (z + t, z + t < levels)):
+
+            @pl.when(there)
+            def _(zz=zz):
+                arrived_across(q, zz).wait_recv()
+                beside(q, zz, 1 - y, c).start()
+
+    def from_partner(q, zz):
+        for hh in range(2):
+            beside(q, zz, hh, 1 - c).wait_recv()
+
+    def project():
+        def tile(j, _):
+            cols = pl.ds(pl.multiple_of(j * 256, 256), 256)
+            psend[:, cols] = jnp.dot(mixed[peer_rows, :], wout[:, cols], preferred_element_type=jnp.float32).astype(jnp.bfloat16)
+            out[:, cols] = jnp.dot(mixed[own_rows, :], wout[:, cols], preferred_element_type=jnp.float32).astype(jnp.bfloat16)
+            return 0
+
+        lax.fori_loop(0, dim // 256, tile, 0)
+
+    def sent_projection():
+        return remote(psend, precv, x_send.at[0], x_recv.at[0], x_peer)
+
+    def sent_normed(rows):
+        return remote(normed.at[rows, :], normed.at[rows, :], x_send.at[1], x_recv.at[1], x_peer)
+
+    step_rows = 32
+
+    def norms():
+        def tile(i, _):
+            rows = pl.ds(pl.multiple_of(i * step_rows, step_rows), step_rows)
+            projected = (out[rows, :].astype(jnp.float32) + precv[rows, :].astype(jnp.float32)).astype(jnp.bfloat16).astype(jnp.float32)
+            total = (resid[rows, :].astype(jnp.float32) + rms_scaled(projected, gain_m[...])).astype(jnp.bfloat16)
+            after[rows, :] = total
+            placed = pl.ds(pl.multiple_of(x * mine + i * step_rows, step_rows), step_rows)
+            normed[placed, :] = rms_scaled(total.astype(jnp.float32), gain_b[...]).astype(jnp.bfloat16)
+            return 0
+
+        lax.fori_loop(0, mine // step_rows, tile, 0)
+
+    tiles = full_gate.shape[1] // 256
+
+    def gathered(w):
+        for hh in range(2):
+            keep(w, hh).wait()
+        for zz in range(levels):
+            from_partner(w, zz)
+
+    def gated(first, last):
+        def tile(j, _):
+            cols = pl.ds(pl.multiple_of(j * 256, 256), 256)
+            g = jnp.dot(normed[...], full_gate[:, cols], preferred_element_type=jnp.float32)
+            hidden[:, cols] = (g / (1.0 + jnp.exp(-g))).astype(jnp.bfloat16)
+            return 0
+
+        lax.fori_loop(first, last, tile, 0)
+
+    def raised(first, last):
+        def tile(j, _):
+            cols = pl.ds(pl.multiple_of(j * 256, 256), 256)
+            u = jnp.dot(normed[...], full_up[:, cols], preferred_element_type=jnp.float32)
+            hidden[:, cols] = (hidden[:, cols].astype(jnp.float32) * u).astype(jnp.bfloat16)
+            return 0
+
+        lax.fori_loop(first, last, tile, 0)
+
+    def sent_sum(k, zz):
+        return remote(fsend.at[k, zz], frecv.at[k, zz], f_send.at[k, zz], f_recv.at[k, zz], x_peer)
+
+    def lowered(k, zz):
+        from_partner(k + 2, zz)
+        block = full_down.at[k, zz]
+        fsend[k, zz] = jnp.dot(hidden[peer_rows, :], block[...], preferred_element_type=jnp.float32).astype(jnp.bfloat16)
+        sent_sum(k, zz).start()
+        fown[k, zz] = jnp.dot(hidden[own_rows, :], block[...], preferred_element_type=jnp.float32).astype(jnp.bfloat16)
+
+    def lowered_ring(k, t):
+        def one(side, _):
+            zz = z - t + 2 * t * side
+
+            @pl.when((zz >= 0) & (zz < levels))
+            def _():
+                lowered(k, zz)
+
+            return 0
+
+        lax.fori_loop(0, 2, one, 0)
+
+    own(0)
+    own(1)
+    project()
+    sent_projection().start()
+    previous = None
+    second_gate = (levels - 1) + min(2, levels - 1) - 1
+    second_up = second_gate + levels - 1
+    last_tick = PHASES * (levels - 1) - 1
+    for q in range(PHASES):
+        for t in range(1, levels):
+            from_line(q, t)
+            if previous is not None:
+                from_side(*previous)
+            previous = (q, t)
+            if q == 0 and t == 1:
+                own(2)
+            if q == 0 and t == min(2, levels - 1):
+                sent_projection().wait()
+                norms()
+                sent_normed(own_rows).start()
+            if q == 1 and t == 1:
+                own(3)
+            tick = q * (levels - 1) + t - 1
+            if tick == second_gate:
+                sent_normed(own_rows).wait_send()
+                sent_normed(peer_rows).wait_recv()
+                gathered(0)
+            if second_gate <= tick < second_up:
+                at, spread = tick - second_gate, second_up - second_gate
+                gated(tiles * at // spread, tiles * (at + 1) // spread)
+            if tick == second_up:
+                gathered(1)
+            if second_up <= tick < last_tick:
+                at, spread = tick - second_up, last_tick - second_up
+                raised(tiles * at // spread, tiles * (at + 1) // spread)
+            if tick == last_tick:
+                for w in (2, 3):
+                    for hh in range(2):
+                        keep(w, hh).wait()
+
+                def first_half(zz, _):
+                    lowered(0, zz)
+                    return 0
+
+                lax.fori_loop(0, levels, first_half, 0)
+                lowered(1, z)
+                for near in range(1, levels - 1):
+                    lowered_ring(1, near)
+    from_side(*previous)
+    lowered_ring(1, levels - 1)
+
+    def drain(zz, _):
+        for k in range(2):
+            sent_sum(k, zz).wait()
+        for q in range(PHASES):
+            for hh in range(2):
+                beside(q, zz, hh, c).wait_send()
+
+            @pl.when((zz <= z) & (z < levels - 1))
+            def _(q=q):
+                upward(q, zz, place(q, zz, c, y)).wait_send()
+
+            @pl.when((zz >= z) & (z > 0))
+            def _(q=q):
+                downward(q, zz, place(q, zz, c, y)).wait_send()
+
+            @pl.when(zz != z)
+            def _(q=q):
+                across(q, zz).wait_send()
+
+        return 0
+
+    lax.fori_loop(0, levels, drain, 0)
+
+    def finish(i, _):
+        rows = pl.ds(pl.multiple_of(i * step_rows, step_rows), step_rows)
+        parts = [
+            fown[k, zz, rows, cc * width : (cc + 1) * width].astype(jnp.float32)
+            + frecv[k, zz, rows, cc * width : (cc + 1) * width].astype(jnp.float32)
+            for zz in range(levels)
+            for cc in range(2)
+            for k in range(2)
+        ]
+        ffn_out = jnp.concatenate(parts, axis=1).astype(jnp.bfloat16).astype(jnp.float32)
+        out[rows, :] = (after[rows, :].astype(jnp.float32) + 0.5 * rms_scaled(ffn_out, gain_a[...])).astype(jnp.bfloat16)
+        return 0
+
+    lax.fori_loop(0, mine // step_rows, finish, 0)
+
+
+def fused(mixed, head_columns, residual, gain_mixed, gain_before, gain_after, gate_weight, up_weight, down_weight):
+    levels = lax.axis_size("sp") // 2
+    rows, dim = mixed.shape[0], residual.shape[1]
+    mine = residual.shape[0]
+    hidden = gate_weight.shape[1]
+    half = down_weight.shape[1] // 2
+    vmem, whole = pl.BlockSpec(memory_space=pltpu.VMEM), pl.BlockSpec(memory_space=pl.ANY)
+    bf16, dma = jnp.bfloat16, pltpu.SemaphoreType.DMA
+    return pl.pallas_call(
+        functools.partial(block_kernel, levels),
+        out_shape=jax.ShapeDtypeStruct((mine, dim), bf16),
+        in_specs=[vmem] * 6 + [whole] * 3,
+        out_specs=vmem,
+        scratch_shapes=[
+            pltpu.VMEM((dim, hidden), bf16),
+            pltpu.VMEM((dim, hidden), bf16),
+            pltpu.VMEM((2, levels, hidden, 2 * half), bf16),
+            pltpu.VMEM((mine, dim), bf16),
+            pltpu.VMEM((mine, dim), bf16),
+            pltpu.VMEM((mine, dim), bf16),
+            pltpu.VMEM((rows, dim), bf16),
+            pltpu.VMEM((rows, hidden), bf16),
+            pltpu.VMEM((2, levels, mine, 2 * half), bf16),
+            pltpu.VMEM((2, levels, mine, 2 * half), bf16),
+            pltpu.VMEM((2, levels, mine, 2 * half), bf16),
+            dma((PHASES, levels)),
+            dma((PHASES, levels)),
+            dma((PHASES, levels)),
+            dma((PHASES, levels)),
+            dma((PHASES, levels)),
+            dma((PHASES, levels, 2)),
+            dma((PHASES, levels, 2)),
+            dma((PHASES, 2)),
+            dma((2,)),
+            dma((2,)),
+            dma((2, levels)),
+            dma((2, levels)),
+        ],
+        compiler_params=pltpu.CompilerParams(collective_id=0, has_side_effects=True, vmem_limit_bytes=67043328),
+    )(
+        mixed, head_columns, residual, gain_mixed[None], gain_before[None], gain_after[None],
+        gate_weight, up_weight, down_weight,
+    )
+
 
 def per_device(
     queries,
@@ -91,6 +435,11 @@
 ):
     mixed = attend(queries, key_rows, value_rows, doc_ids, sink_logits)
     head_columns = lax.all_gather(out_weight, "sp", axis=1, tiled=True)
+    pairs = lax.axis_size("grp") == 2 and lax.axis_size("tp") == 2
+    if pairs and lax.axis_size("sp") % 2 == 0 and lax.axis_size("sp") >= 4:
+        return fused(
+            mixed, head_columns, residual, gain_mixed, gain_before, gain_after, gate_weight, up_weight, down_weight
+        )
     projected = lax.psum_scatter(
         jnp.dot(mixed, head_columns, preferred_element_type=jnp.float32).astype(jnp.bfloat16),
         "tp",

time: 578 us -> 286 us (0.49)
  waiting for transfers between devices: 469 us -> 3.68 us
  Pallas kernels: 0 us -> 233 us
  matrix products: 56.5 us -> 3.89 us
  other arithmetic: 15.1 us -> 3.88 us
    all_gather x4 -> x0, waiting for transfers between devices: 379 us -> none  [the longest x1 118 us: per_device(): lax.all_gather(gate_weight, 'sp', axis=0, tiled=True)]
    pallas_call x0 -> x1, Pallas kernels: none -> 233 us  [fused(): pl.pallas_call(functools.partial(block_kernel, levels), out_shape=jax.Sha...]
    reduce_scatter x2 -> x0, waiting for transfers between devices: 84 us -> none  [the longest x1 42.3 us: per_device(): lax.psum_scatter(jnp.dot(mixed, head_columns, preferred_element_type=jnp....]
    dot_general x3 -> x0, matrix products: 52.6 us -> none  [the longest x1 31.5 us: per_device(): jnp.dot(hidden, full_down, preferred_element_type=jnp.float32)]
    convert_element_type x3 -> x0, other arithmetic: 7.2 us -> none  [the longest x1 3.39 us: per_device(): return (after + 0.5 * rms_scaled(ffn_out, gain_after)).astype(jnp.bfloat16)]
  transfers between devices with their start and end apart: 10 -> 4, of which waited for: 7 -> 1; matrix products, arithmetic and copies ran while one was open for 6% -> 8% of each run, Pallas kernels for 0% -> 0%
where the time goes in v1:
time: 286 us; the launch traced here: 285 us
  Pallas kernels  233 us (81%)
  local copies, waits for them, and re-layouts  17.8 us (6%)
  between operations  13.6 us (5%)
  starting transfers between devices  8.88 us (3%)
  matrix products  3.89 us (1%)
  other arithmetic  3.88 us (1%)
  waiting for transfers between devices  3.68 us (1%)
    pallas_call x1, Pallas kernels, fused(): pl.pallas_call(functools.partial(block_kernel, levels), out_shape=jax.Sha...  233 us
    ppermute x3, starting transfers between devices, passed_along(): lax.ppermute(value, axis, [(source, source + steps) for source in range(f...  8.88 us
    concatenate x8, local copies, waits for them, and re-layouts, windows(): return jnp.concatenate([first, second], axis=1)  8.06 us
  transfers between devices with their start and end apart: 4, of which 1 were waited for; matrix products, arithmetic and copies ran while one was open for 8% of the time, Pallas kernels for 0%

profile of v1, /device:TPU:0, one launch (start us, length us, event | category | flops | bytes accessed | tf_op | source)
XLA Modules:
  0.0 285.1 jit_solution(950706369259637708)
XLA Ops:
  6.5 0.0 copy-start.3
  6.5 0.0 all-gather.2.cloned.1.call-start
  6.5 0.7 all-gather.2.cloned.1.call-update
  7.3 0.0 copy-start.7
  7.3 0.7 slice.40
  8.0 2.4 collective-permute-start.1
  10.4 0.8 slice.43
  11.2 5.2 %collective-permute-start.2 = (bf16[128,256]{1,0:T(8,128)(2,1)S(1)}, bf16[128,256]{1,0:T(8,128)(2,1)}, u32[]{:S(2)}, u32[]{:S(2)}) collective-permute-start(bf16[128,256]{1,0:T(8,128)(2,1)S(1)} %slice.43), channel_id=1, source_target_pairs={{0,2},{2,4},{4,6},{6,8},{8,10},{10,12},{12,14},{1,3},{3,5},{5,7},{... | collective-permute-start | bytes 196616 | tf_op jit(solution)/shard_map/ppermute | solution.py:21
  16.4 0.8 slice.36
  17.2 1.3 collective-permute-start
  18.6 1.8 reshape.80
  20.5 0.0 copy-start.6
  20.5 0.0 copy-start
  20.5 1.9 reshape.78
  22.4 0.0 copy-done.3
  22.4 1.7 reshape.81
  24.1 0.0 copy-start.1
  24.1 1.1 copy.24
  25.2 0.0 copy-done.7
  25.2 0.1 max.16
  25.3 1.1 copy.20
  26.3 0.0 collective-permute-done.1
  26.4 0.0 copy-done.6
  26.4 1.0 fusion.20
  27.4 0.0 copy-start.2
  27.4 0.0 collective-permute-done.2
  27.4 0.0 copy-done
  27.4 1.0 pad_maximum_fusion
  28.4 0.3 reshape.79
  28.7 0.0 copy-start.5
  28.7 1.1 copy.23
  29.8 0.0 collective-permute-done
  29.8 0.0 copy-done.1
  29.8 0.3 reshape.77
  30.1 0.5 copy.19
  30.6 0.0 copy-done.2
  30.6 0.0 copy-done.5
  30.6 2.3 fusion.2
  32.9 0.1 broadcast_maximum_fusion
  33.0 0.0 copy-start.4
  33.0 1.7 fusion
  34.7 0.1 add_bitcast_fusion
  34.8 0.0 copy-done.4
  34.8 1.6 fusion.9
  36.4 1.2 copy.43
  37.6 1.7 reshape.82.mixed
  39.3 3.0 %all-gather.2.cloned.1.call-done.wout = bf16[512,2048]{1,0:T(8,128)(2,1)} async-done(((bf16[512,256]{1,0:T(8,128)(2,1)}), bf16[512,2048]{1,0:T(8,128)(2,1)}) %all-gather.2.cloned.1.call-update) | async-done | bytes 2097168 | tf_op jit(solution)/shard_map/all_gather | solution.py:437
  42.2 233.3 %shard_map.127 = bf16[384,2048]{1,0:T(8,128)(2,1)} custom-call(bf16[768,512]{1,0:T(8,128)(2,1)} %reshape.82.mixed, bf16[512,2048]{1,0:T(8,128)(2,1)} %all-gather.2.cloned.1.call-done.wout, bf16[384,2048]{1,0:T(8,128)(2,1)} %resid.1, f32[1,2048]{1,0:T(1,128)} %bitcast.37, f32[1,2048]{1,0:T(1,128)} %bitcast.38, f32[1,2048]{1,0:T(1,128)} %bitcast.39, ...), custom_call_target="tpu_custom_call" | custom-call | tf_op jit(solution)/shard_map/pallas_call | solution.py:384
  275.6 2.7 copy.50
  (8 shorter events, 0.1 us)
Async XLA Ops:
  6.5 15.8 %copy-start.3 = (bf16[768,512]{1,0:T(8,128)(2,1)S(1)}, bf16[768,512]{1,0:T(8,128)(2,1)}, u32[]{:S(2)}) copy-start(bf16[768,512]{1,0:T(8,128)(2,1)} %param.13) | copy-start | bytes 2359300
  6.5 35.7 %all-gather.2.cloned.1.call-start = ((), (), s32[]{:S(2)}) async-start(), calls=%async_computation | async-start | bytes 2359296 | tf_op jit(solution)/shard_map/all_gather | solution.py:437
  7.3 17.9 %copy-start.7 = (f32[8]{0:T(128)S(1)}, f32[8]{0:T(128)}, u32[]{:S(2)}) copy-start(f32[8]{0:T(128)} %param.17) | copy-start | bytes 100
  8.0 18.4 %collective-permute-start.1 = (s32[128]{0:T(128)S(1)}, s32[128]{0:T(128)S(1)}, u32[]{:S(2)}, u32[]{:S(2)}) collective-permute-start(s32[128]{0:T(128)S(1)} %slice.40), channel_id=1, source_target_pairs={{0,2},{2,4},{4,6},{6,8},{8,10},{10,12},{12,14},{1,3},{3,5},{5,7},{... | collective-permute-start | bytes 1544 | tf_op jit(solution)/shard_map/ppermute | solution.py:21
  11.2 16.2 %collective-permute-start.2 = (bf16[128,256]{1,0:T(8,128)(2,1)S(1)}, bf16[128,256]{1,0:T(8,128)(2,1)}, u32[]{:S(2)}, u32[]{:S(2)}) collective-permute-start(bf16[128,256]{1,0:T(8,128)(2,1)S(1)} %slice.43), channel_id=1, source_target_pairs={{0,2},{2,4},{4,6},{6,8},{8,10},{10,12},{12,14},{1,3},{3,5},{5,7},{... | collective-permute-start | bytes 196616 | tf_op jit(solution)/shard_map/ppermute | solution.py:21
  17.2 12.5 %collective-permute-start = (bf16[128,256]{1,0:T(8,128)(2,1)S(1)}, bf16[128,256]{1,0:T(8,128)(2,1)S(1)}, u32[]{:S(2)}, u32[]{:S(2)}) collective-permute-start(bf16[128,256]{1,0:T(8,128)(2,1)S(1)} %slice.36), channel_id=1, source_target_pairs={{0,2},{2,4},{4,6},{6,8},{8,10},{10,12},{12,14},{1,3},{3,5},{5,7},{... | collective-permute-start | bytes 196616 | tf_op jit(solution)/shard_map/ppermute | solution.py:21
  20.5 5.9 %copy-start.6 = (s32[768]{0:T(1024)S(1)}, s32[768]{0:T(1024)}, u32[]{:S(2)}) copy-start(s32[768]{0:T(1024)} %param.16) | copy-start | bytes 9220
  20.5 6.9 %copy-start = (bf16[768,256]{1,0:T(8,128)(2,1)S(1)}, bf16[768,256]{1,0:T(8,128)(2,1)}, u32[]{:S(2)}) copy-start(bf16[768,256]{1,0:T(8,128)(2,1)} %param.14) | copy-start | bytes 1179652
  24.1 5.7 %copy-start.1 = (bf16[768,256]{1,0:T(8,128)(2,1)S(1)}, bf16[768,256]{1,0:T(8,128)(2,1)}, u32[]{:S(2)}) copy-start(bf16[768,256]{1,0:T(8,128)(2,1)} %param.15) | copy-start | bytes 1179652
  27.4 3.3 %copy-start.2 = (bf16[6,128,4,2,64]{4,3,2,1,0:T(2,128)(2,1)S(1)}, bf16[6,128,4,2,64]{4,3,2,1,0:T(2,128)(2,1)}, u32[]{:S(2)}) copy-start(bf16[6,128,4,2,64]{4,3,2,1,0:T(2,128)(2,1)} %reshape.81) | copy-start | bytes 2359300
  28.7 1.9 copy-start.5
  33.0 1.8 copy-start.4
Sparse Core Ops, SparseCore 0:
  8.9 33.2 all-gather.1
